TPU v7x, 32 devices: a whole 2x2x4 slice. The times are simulated.
32 devices in a mesh: tp: 16 (over z, y, core), dp: 2 (over x).
Axes of the slice: x: 2, y: 2, z: 4, core: 2. Of those that a mesh axis runs over, the one named last changes fastest.
Arguments:
- resid: bfloat16 [64, 2048], P('dp', 'tp'), may hold values from -6 to 6
- norm_gain: float32 [2, 2048], replicated, may hold values from 0.1 to 1.9
- w_query: bfloat16 [2, 2048, 2048], P(None, 'dp', 'tp'), may hold values from -0.125 to 0.125
- w_forget: bfloat16 [2, 2048, 2048], P(None, 'dp', 'tp'), may hold values from -0.125 to 0.125
- w_value: bfloat16 [2, 2048, 16, 128], P(None, 'dp', None, 'tp'), may hold values from -0.125 to 0.125
- w_gate: bfloat16 [2, 2048, 16, 128], P(None, 'dp', None, 'tp'), may hold values from -0.125 to 0.125
- gate_floor: float32 [2, 2048], replicated, may hold values from 0 to 0.9
- states: float32 [2, 64, 16, 128, 128], P(None, 'dp', None, 'tp'), may hold values from -1 to 1
- out_gain: float32 [2, 16, 128], P(None, None, 'tp'), may hold values from 0.1 to 1.9
- w_out: bfloat16 [2, 16, 128, 2048], P(None, None, 'tp'), may hold values from -0.125 to 0.125
Outputs:
- new_resid: bfloat16 [64, 2048], P('dp', 'tp')
- new_states: float32 [2, 64, 16, 128, 128], P(None, 'dp', None, 'tp')
All inputs are finite; a program needn't handle non-finite values.
Results may differ from a plain program's by a relative error of at most 0.029.
Values may be sent and summed in bfloat16 or wider, within the bound.
No kernel may reach another device: no remote copies, remote signals or barrier semaphores. Data moves between devices by JAX's collectives and lax.ppermute only.
A program may use at most 64 MiB of HBM per device.

v0:
```python
import jax
import jax.numpy as jnp
from jax import lax
from jax.sharding import PartitionSpec as P

BLOCKS = 2
epsilon = 1e-06


def shards(
    resid, norm_gain, w_query, w_forget, w_value, w_gate, gate_floor, states, out_gain, w_out
):
    residual = resid
    seq_local = resid.shape[0]
    heads = states.shape[2]
    slice_cols = states.shape[3]
    head_dim = states.shape[4]
    row_count = w_query.shape[1]
    new_list = []
    for layer in range(BLOCKS):
        gathered = lax.all_gather(residual, "tp", axis=1, tiled=True)
        resid_f32 = gathered.astype(jnp.float32)
        inv_rms = lax.rsqrt(jnp.mean(resid_f32 * resid_f32, axis=1, keepdims=True) + epsilon)
        scaled = (resid_f32 * norm_gain[layer]).astype(jnp.bfloat16)
        query_rows = w_query[layer]
        forget_rows = w_forget[layer]
        value_rows = w_value[layer].reshape(row_count, -1)
        gate_rows = w_gate[layer].reshape(row_count, -1)
        zero_sums = (
            jnp.zeros((seq_local, query_rows.shape[1]), jnp.float32),
            jnp.zeros((seq_local, forget_rows.shape[1]), jnp.float32),
            jnp.zeros((seq_local, value_rows.shape[1]), jnp.float32),
            jnp.zeros((seq_local, gate_rows.shape[1]), jnp.float32),
        )
        totals = zero_sums
        pieces = (
            lax.all_gather(query_rows, "dp", axis=0, tiled=True),
            lax.all_gather(forget_rows, "dp", axis=0, tiled=True),
            lax.all_gather(value_rows, "dp", axis=0, tiled=True),
            lax.all_gather(gate_rows, "dp", axis=0, tiled=True),
        )
        segments = pieces[0].shape[0] // row_count
        for part_index in range(segments):
            columns = lax.dynamic_slice_in_dim(scaled, part_index * row_count, row_count, 1)
            lo_row = part_index * row_count
            totals = tuple(
                (
                    total
                    + lax.optimization_barrier(
                        jnp.dot(
                            columns,
                            segment[lo_row : lo_row + row_count],
                            preferred_element_type=jnp.float32,
                        ).astype(jnp.bfloat16)
                    ).astype(jnp.float32)
                    for total, segment in zip(totals, pieces)
                )
            )
        queries, forget_pre, values, gate_pre = [
            (summed * inv_rms).astype(jnp.bfloat16) for summed in totals
        ]
        query_all, forget_all = (
            lax.all_gather(queries, "tp", axis=1, tiled=True),
            lax.all_gather(forget_pre, "tp", axis=1, tiled=True),
        )
        floor_now = gate_floor[layer]
        keep = floor_now + (1.0 - floor_now) * jax.nn.sigmoid(forget_all.astype(jnp.float32))
        keep = keep.reshape(seq_local, heads, head_dim)
        value_f32 = values.astype(jnp.float32).reshape(seq_local, heads, slice_cols)
        state_new = (
            keep[:, :, None, :] * states[layer]
            + (1.0 - keep)[:, :, None, :] * value_f32[:, :, :, None]
        )
        query_f32 = query_all.astype(jnp.float32).reshape(seq_local, heads, head_dim)
        readout = jnp.sum(query_f32[:, :, None, :] * state_new, axis=3)
        power_sum = lax.psum(jnp.sum(readout * readout, axis=2), "tp")
        mean_square = power_sum[..., None] / head_dim
        gate_f32 = gate_pre.astype(jnp.float32).reshape(seq_local, heads, slice_cols)
        normed = (
            readout * lax.rsqrt(mean_square + epsilon) * out_gain[layer] * jax.nn.silu(gate_f32)
        ).astype(jnp.bfloat16)
        flattened = normed.reshape(seq_local, heads * slice_cols)
        weight_out = w_out[layer].reshape(heads * slice_cols, -1)
        branch = lax.psum_scatter(
            lax.dot_general(
                weight_out, flattened, (((0,), (1,)), ((), ())), preferred_element_type=jnp.float32
            ),
            "tp",
            scatter_dimension=0,
            tiled=True,
        )
        residual = (residual.astype(jnp.float32) + branch.T).astype(jnp.bfloat16)
        new_list.append(state_new)
    return (residual, jnp.stack(new_list))


def solution(mesh):
    return jax.shard_map(
        shards,
        mesh=mesh,
        in_specs=(
            P("dp", "tp"),
            P(),
            P(None, "dp", "tp"),
            P(None, "dp", "tp"),
            P(None, "dp", None, "tp"),
            P(None, "dp", None, "tp"),
            P(),
            P(None, "dp", None, "tp", None),
            P(None, None, "tp"),
            P(None, None, "tp", None),
        ),
        out_specs=(P("dp", "tp"), P(None, "dp", None, "tp", None)),
        check_vma=False,
    )
```

profile of v0, /device:TPU:0, one launch (start us, length us, event | category | flops | bytes accessed | tf_op | source)
XLA Modules:
  0.0 405.7 jit_solution(406525206643660046)
XLA Ops:
  8.0 23.7 %all_gather.42 = bf16[32,2048]{1,0:T(8,128)(2,1)S(1)} all-gather(bf16[32,128]{1,0:T(8,128)(2,1)} %param.10), channel_id=1, replica_groups=mesh['tp'=16,'dp'=2] {'tp'}, dimensions={1}, use_global_device_ids=true | all-gather | bytes 139264 | tf_op jit(solution)/shard_map/all_gather | solution.py:21
  32.8 9.4 %all-gather = bf16[1,2048,128]{2,1,0:T(8,128)(2,1)S(1)} all-gather(bf16[1,1024,128]{2,1,0:T(8,128)(2,1)S(1)} %get-tuple-element.7), channel_id=2, replica_groups=mesh['tp'=16,'dp'=2] {'dp'}, dimensions={1}, use_global_device_ids=true | all-gather | bytes 786432 | tf_op jit(solution)/shard_map/all_gather | solution.py:37
  42.7 8.5 %all-gather.1 = bf16[1,2048,128]{2,1,0:T(8,128)(2,1)S(1)} all-gather(bf16[1,1024,128]{2,1,0:T(8,128)(2,1)S(1)} %get-tuple-element.9), channel_id=3, replica_groups=mesh['tp'=16,'dp'=2] {'dp'}, dimensions={1}, use_global_device_ids=true | all-gather | bytes 786432 | tf_op jit(solution)/shard_map/all_gather | solution.py:38
  51.7 7.5 %all_gather.47 = bf16[2048,128]{0,1:T(8,128)(2,1)S(1)} all-gather(bf16[1024,128]{0,1:T(8,128)(2,1)S(1)} %get-tuple-element.10), channel_id=1, replica_groups=mesh['tp'=16,'dp'=2] {'dp'}, dimensions={0}, use_global_device_ids=true | all-gather | bytes 786432 | tf_op jit(solution)/shard_map/all_gather | solution.py:39
  59.6 7.0 %all_gather.48 = bf16[2048,128]{0,1:T(8,128)(2,1)S(1)} all-gather(bf16[1024,128]{0,1:T(8,128)(2,1)S(1)} %get-tuple-element.5), channel_id=1, replica_groups=mesh['tp'=16,'dp'=2] {'dp'}, dimensions={0}, use_global_device_ids=true | all-gather | bytes 786432 | tf_op jit(solution)/shard_map/all_gather | solution.py:40
  67.5 17.5 %all_gather.44 = bf16[32,2048]{1,0:T(8,128)(2,1)S(1)} all-gather(bf16[32,128]{1,0:T(8,128)(2,1)S(1)} %get-tuple-element.27), channel_id=1, replica_groups=mesh['tp'=16,'dp'=2] {'tp'}, dimensions={1}, use_global_device_ids=true | all-gather | bytes 139264 | tf_op jit(solution)/shard_map/all_gather | solution.py:63
  85.0 19.4 %all_gather.46 = bf16[32,2048]{1,0:T(8,128)(2,1)S(1)} all-gather(bf16[32,128]{1,0:T(8,128)(2,1)S(1)} %get-tuple-element.28), channel_id=1, replica_groups=mesh['tp'=16,'dp'=2] {'tp'}, dimensions={1}, use_global_device_ids=true | all-gather | bytes 139264 | tf_op jit(solution)/shard_map/all_gather | solution.py:64
  104.8 2.6 fusion.5
  107.6 57.8 %psum.14 = f32[32,16]{1,0:T(8,128)S(1)} all-reduce(f32[32,16]{1,0:T(8,128)S(1)} %multiply_reduce_fusion.1), channel_id=1, replica_groups=mesh['tp'=16,'dp'=2] {'tp'}, use_global_device_ids=true, to_apply=%region_3.0 | all-reduce | flops 512 | bytes 4096 | tf_op jit(solution)/shard_map/psum | solution.py:76
  167.0 9.5 %all-gather.2 = bf16[1,2048,128]{2,1,0:T(8,128)(2,1)} all-gather(bf16[1,1024,128]{2,1,0:T(8,128)(2,1)S(1)} %get-tuple-element.6), channel_id=4, replica_groups=mesh['tp'=16,'dp'=2] {'dp'}, dimensions={1}, use_global_device_ids=true | all-gather | bytes 786432 | tf_op jit(solution)/shard_map/all_gather | solution.py:37
  176.5 9.2 %all-gather.3 = bf16[1,2048,128]{2,1,0:T(8,128)(2,1)S(1)} all-gather(bf16[1,1024,128]{2,1,0:T(8,128)(2,1)S(1)} %get-tuple-element.8), channel_id=5, replica_groups=mesh['tp'=16,'dp'=2] {'dp'}, dimensions={1}, use_global_device_ids=true | all-gather | bytes 786432 | tf_op jit(solution)/shard_map/all_gather | solution.py:38
  185.7 8.4 %all_gather.54 = bf16[2048,128]{0,1:T(8,128)(2,1)} all-gather(bf16[1024,128]{0,1:T(8,128)(2,1)S(1)} %get-tuple-element.11), channel_id=1, replica_groups=mesh['tp'=16,'dp'=2] {'dp'}, dimensions={0}, use_global_device_ids=true | all-gather | bytes 786432 | tf_op jit(solution)/shard_map/all_gather | solution.py:39
  194.1 7.1 %all_gather.55 = bf16[2048,128]{0,1:T(8,128)(2,1)} all-gather(bf16[1024,128]{0,1:T(8,128)(2,1)S(1)} %get-tuple-element.4), channel_id=1, replica_groups=mesh['tp'=16,'dp'=2] {'dp'}, dimensions={0}, use_global_device_ids=true | all-gather | bytes 786432 | tf_op jit(solution)/shard_map/all_gather | solution.py:40
  201.3 18.7 %reduce-scatter.3.cloned.1.call-done = f32[128,32]{0,1:T(8,128)} async-done(((f32[2048,32]{0,1:T(8,128)}), f32[128,32]{0,1:T(8,128)}) %reduce-scatter.3.cloned.1.call-update) | async-done | bytes 16400 | tf_op jit(solution)/shard_map/reduce_scatter | solution.py:84
  220.7 19.7 %all_gather.49 = bf16[32,2048]{1,0:T(8,128)(2,1)S(1)} all-gather(bf16[32,128]{1,0:T(8,128)(2,1)S(1)} %fusion.47), channel_id=1, replica_groups=mesh['tp'=16,'dp'=2] {'tp'}, dimensions={1}, use_global_device_ids=true | all-gather | bytes 139264 | tf_op jit(solution)/shard_map/all_gather | solution.py:21
  242.1 1.2 convolution_convert_fusion.2
  245.2 17.8 %all_gather.51 = bf16[32,2048]{1,0:T(8,128)(2,1)S(1)} all-gather(bf16[32,128]{1,0:T(8,128)(2,1)S(1)} %get-tuple-element.24), channel_id=1, replica_groups=mesh['tp'=16,'dp'=2] {'tp'}, dimensions={1}, use_global_device_ids=true | all-gather | bytes 139264 | tf_op jit(solution)/shard_map/all_gather | solution.py:63
  263.0 19.1 %all_gather.53 = bf16[32,2048]{1,0:T(8,128)(2,1)S(1)} all-gather(bf16[32,128]{1,0:T(8,128)(2,1)S(1)} %get-tuple-element.25), channel_id=1, replica_groups=mesh['tp'=16,'dp'=2] {'tp'}, dimensions={1}, use_global_device_ids=true | all-gather | bytes 139264 | tf_op jit(solution)/shard_map/all_gather | solution.py:64
  282.5 2.6 fusion.2
  285.2 57.8 %psum.15 = f32[32,16]{1,0:T(8,128)S(1)} all-reduce(f32[32,16]{1,0:T(8,128)S(1)} %multiply_reduce_fusion), channel_id=1, replica_groups=mesh['tp'=16,'dp'=2] {'tp'}, use_global_device_ids=true, to_apply=%region_8.9 | all-reduce | flops 512 | bytes 4096 | tf_op jit(solution)/shard_map/psum | solution.py:76
  344.4 3.5 multiply_add_fusion.1
  348.0 2.3 pad_maximum_fusion
  350.2 47.3 %reduce-scatter.5.cloned.1.call-done = f32[128,32]{0,1:T(8,128)} async-done(((f32[2048,32]{0,1:T(8,128)}), f32[128,32]{0,1:T(8,128)}) %reduce-scatter.5.cloned.1.call-update) | async-done | bytes 16400 | tf_op jit(solution)/shard_map/reduce_scatter | solution.py:84
  397.5 1.3 fusion.46
  (81 shorter events, 12.2 us)
Async XLA Ops:
  7.2 35.5 %copy-start.3 = (bf16[2,1024,128]{2,1,0:T(8,128)(2,1)S(1)}, bf16[2,1024,128]{2,1,0:T(8,128)(2,1)}, u32[]{:S(2)}) copy-start(bf16[2,1024,128]{2,1,0:T(8,128)(2,1)} %param.13) | copy-start | bytes 1572868
  7.2 212.8 %reduce-scatter.3.cloned.1.call-start = ((), (), s32[]{:S(2)}) async-start(), calls=%async_computation.2 | async-start | bytes 278528 | tf_op jit(solution)/shard_map/reduce_scatter | solution.py:84
  32.8 18.8 %copy-start.4 = (bf16[2,1024,16,8]{1,3,2,0:T(8,128)(2,1)S(1)}, bf16[2,1024,16,8]{1,3,2,0:T(8,128)(2,1)}, u32[]{:S(2)}) copy-start(bf16[2,1024,16,8]{1,3,2,0:T(8,128)(2,1)} %param.14) | copy-start | bytes 1572868
  42.7 16.8 %copy-start.5 = (bf16[2,1024,16,8]{1,3,2,0:T(8,128)(2,1)S(1)}, bf16[2,1024,16,8]{1,3,2,0:T(8,128)(2,1)}, u32[]{:S(2)}) copy-start(bf16[2,1024,16,8]{1,3,2,0:T(8,128)(2,1)} %param.15) | copy-start | bytes 1572868
  51.6 15.4 %copy-start.8 = (f32[2,16,8]{1,2,0:T(8,128)S(1)}, f32[2,16,8]{1,2,0:T(8,128)}, u32[]{:S(2)}) copy-start(f32[2,16,8]{1,2,0:T(8,128)} %param.18) | copy-start | bytes 3076
  51.6 15.6 %copy-start.7 = (f32[2,2048]{1,0:T(2,128)S(1)}, f32[2,2048]{1,0:T(2,128)}, u32[]{:S(2)}) copy-start(f32[2,2048]{1,0:T(2,128)} %param.16) | copy-start | bytes 49156
  104.8 61.0 %copy-start = (bf16[2,16,8,2048]{3,2,1,0:T(8,128)(2,1)S(1)}, bf16[2,16,8,2048]{3,2,1,0:T(8,128)(2,1)}, u32[]{:S(2)}) copy-start(bf16[2,16,8,2048]{3,2,1,0:T(8,128)(2,1)} %param.19) | copy-start | bytes 3145732
  165.8 54.2 %copy-start.6 = (bf16[32,128]{1,0:T(8,128)(2,1)S(1)}, bf16[32,128]{1,0:T(8,128)(2,1)}, u32[]{:S(2)}) copy-start(bf16[32,128]{1,0:T(8,128)(2,1)} %param.10) | copy-start | bytes 24580
  166.8 230.7 %reduce-scatter.5.cloned.1.call-start = ((), (), s32[]{:S(2)}) async-start(), calls=%async_computation.3 | async-start | bytes 278528 | tf_op jit(solution)/shard_map/reduce_scatter | solution.py:84
  185.7 58.9 %copy-start.1 = (bf16[1,2048,128]{2,1,0:T(8,128)(2,1)S(1)}, bf16[1,2048,128]{2,1,0:T(8,128)(2,1)}, u32[]{:S(2)}) copy-start(bf16[1,2048,128]{2,1,0:T(8,128)(2,1)} %all-gather.2) | copy-start | bytes 1572868
  201.3 43.1 %copy-start.2 = (bf16[2048,128]{0,1:T(8,128)(2,1)S(1)}, bf16[2048,128]{0,1:T(8,128)(2,1)}, u32[]{:S(2)}) copy-start(bf16[2048,128]{0,1:T(8,128)(2,1)} %all_gather.55) | copy-start | bytes 1572868
Sparse Core Ops, SparseCore 0:
  166.9 52.9 reduce-scatter.2
  344.5 52.9 reduce-scatter.4
where the time goes:
time: 406 us
  blocking collectives  300 us (74%)
  waiting for transfers between devices  66 us (16%)
  other arithmetic  14.4 us (4%)
  between operations  14.4 us (4%)
  matrix products  7.68 us (2%)
    psum x2, blocking collectives, shards(): power_sum = lax.psum(jnp.sum(readout * readout, axis=2), 'tp')  116 us
    reduce_scatter x2, waiting for transfers between devices, shards(): lax.psum_scatter(lax.dot_general(weight_out, flattened, (((0,), (1,)), ((...  66 us
    all_gather x2, blocking collectives, shards(): gathered = lax.all_gather(residual, 'tp', axis=1, tiled=True)  43.5 us
    all_gather x2, blocking collectives, shards(): lax.all_gather(forget_pre, 'tp', axis=1, tiled=True)  38.5 us
    all_gather x2, blocking collectives, shards(): lax.all_gather(queries, 'tp', axis=1, tiled=True)  35.3 us
    all_gather x2, blocking collectives, shards(): lax.all_gather(query_rows, 'dp', axis=0, tiled=True)  18.8 us
    all_gather x2, blocking collectives, shards(): lax.all_gather(forget_rows, 'dp', axis=0, tiled=True)  17.7 us
    all_gather x2, blocking collectives, shards(): lax.all_gather(value_rows, 'dp', axis=0, tiled=True)  15.9 us
  transfers between devices with their start and end apart: 2, of which 2 were waited for; matrix products, arithmetic and copies ran while one was open for 1% of the time, Pallas kernels for 0%

commit v1 on v0

--- a/solution.py
+++ b/solution.py
@@ -73,7 +73,7 @@
         )
         query_f32 = query_all.astype(jnp.float32).reshape(seq_local, heads, head_dim)
         readout = jnp.sum(query_f32[:, :, None, :] * state_new, axis=3)
-        power_sum = lax.psum(jnp.sum(readout * readout, axis=2), "tp")
+        power_sum = jnp.sum(lax.all_gather(jnp.sum(readout * readout, axis=2), "tp"), axis=0)
         mean_square = power_sum[..., None] / head_dim
         gate_f32 = gate_pre.astype(jnp.float32).reshape(seq_local, heads, slice_cols)
         normed = (

time: 406 us -> 329 us (0.81)
  blocking collectives: 300 us -> 218 us
    psum x2 -> x0, blocking collectives: 116 us -> none  [shards(): power_sum = lax.psum(jnp.sum(readout * readout, axis=2), 'tp')]
    all_gather x0 -> x2, blocking collectives: none -> 35.6 us  [shards(): lax.all_gather(jnp.sum(readout * readout, axis=2), 'tp')]
  transfers between devices with their start and end apart: 2 -> 2, of which waited for: 2 -> 2; matrix products, arithmetic and copies ran while one was open for 1% -> 2% of each run, Pallas kernels for 0% -> 0%
where the time goes in v1:
time: 329 us; the launch traced here: 328 us
  blocking collectives  218 us (66%)
  waiting for transfers between devices  69.9 us (21%)
  between operations  14.4 us (4%)
  other arithmetic  14.2 us (4%)
  matrix products  7.67 us (2%)
  local copies, waits for them, and re-layouts  4.01 us (1%)
    reduce_scatter x2, waiting for transfers between devices, shards(): lax.psum_scatter(lax.dot_general(weight_out, flattened, (((0,), (1,)), ((...  69.9 us
    all_gather x2, blocking collectives, shards(): gathered = lax.all_gather(residual, 'tp', axis=1, tiled=True)  43.5 us
    all_gather x2, blocking collectives, shards(): lax.all_gather(forget_pre, 'tp', axis=1, tiled=True)  38.5 us
    all_gather x2, blocking collectives, shards(): lax.all_gather(jnp.sum(readout * readout, axis=2), 'tp')  35.6 us
    all_gather x2, blocking collectives, shards(): lax.all_gather(queries, 'tp', axis=1, tiled=True)  35.3 us
    all_gather x2, blocking collectives, shards(): lax.all_gather(query_rows, 'dp', axis=0, tiled=True)  18.7 us
    all_gather x2, blocking collectives, shards(): lax.all_gather(forget_rows, 'dp', axis=0, tiled=True)  16.8 us
    all_gather x2, blocking collectives, shards(): lax.all_gather(value_rows, 'dp', axis=0, tiled=True)  15.2 us
  transfers between devices with their start and end apart: 2, of which 2 were waited for; matrix products, arithmetic and copies ran while one was open for 2% of the time, Pallas kernels for 0%

profile of v1, /device:TPU:0, one launch (start us, length us, event | category | flops | bytes accessed | tf_op | source)
XLA Modules:
  0.0 328.1 jit_solution(10134821384057871304)
XLA Ops:
  8.0 23.7 %all_gather.54 = bf16[32,2048]{1,0:T(8,128)(2,1)S(1)} all-gather(bf16[32,128]{1,0:T(8,128)(2,1)} %param.10), channel_id=1, replica_groups=mesh['tp'=16,'dp'=2] {'tp'}, dimensions={1}, use_global_device_ids=true | all-gather | bytes 139264 | tf_op jit(solution)/shard_map/all_gather | solution.py:21
  32.8 9.4 %all-gather = bf16[1,2048,128]{2,1,0:T(8,128)(2,1)S(1)} all-gather(bf16[1,1024,128]{2,1,0:T(8,128)(2,1)S(1)} %get-tuple-element.7), channel_id=2, replica_groups=mesh['tp'=16,'dp'=2] {'dp'}, dimensions={1}, use_global_device_ids=true | all-gather | bytes 786432 | tf_op jit(solution)/shard_map/all_gather | solution.py:37
  42.7 8.5 %all-gather.1 = bf16[1,2048,128]{2,1,0:T(8,128)(2,1)S(1)} all-gather(bf16[1,1024,128]{2,1,0:T(8,128)(2,1)S(1)} %get-tuple-element.9), channel_id=3, replica_groups=mesh['tp'=16,'dp'=2] {'dp'}, dimensions={1}, use_global_device_ids=true | all-gather | bytes 786432 | tf_op jit(solution)/shard_map/all_gather | solution.py:38
  51.7 7.5 %all_gather.59 = bf16[2048,128]{0,1:T(8,128)(2,1)S(1)} all-gather(bf16[1024,128]{0,1:T(8,128)(2,1)S(1)} %get-tuple-element.10), channel_id=1, replica_groups=mesh['tp'=16,'dp'=2] {'dp'}, dimensions={0}, use_global_device_ids=true | all-gather | bytes 786432 | tf_op jit(solution)/shard_map/all_gather | solution.py:39
  59.6 7.0 %all_gather.62 = bf16[2048,128]{0,1:T(8,128)(2,1)S(1)} all-gather(bf16[1024,128]{0,1:T(8,128)(2,1)S(1)} %get-tuple-element.5), channel_id=1, replica_groups=mesh['tp'=16,'dp'=2] {'dp'}, dimensions={0}, use_global_device_ids=true | all-gather | bytes 786432 | tf_op jit(solution)/shard_map/all_gather | solution.py:40
  67.5 17.5 %all_gather.56 = bf16[32,2048]{1,0:T(8,128)(2,1)S(1)} all-gather(bf16[32,128]{1,0:T(8,128)(2,1)S(1)} %get-tuple-element.27), channel_id=1, replica_groups=mesh['tp'=16,'dp'=2] {'tp'}, dimensions={1}, use_global_device_ids=true | all-gather | bytes 139264 | tf_op jit(solution)/shard_map/all_gather | solution.py:63
  85.0 19.4 %all_gather.58 = bf16[32,2048]{1,0:T(8,128)(2,1)S(1)} all-gather(bf16[32,128]{1,0:T(8,128)(2,1)S(1)} %get-tuple-element.28), channel_id=1, replica_groups=mesh['tp'=16,'dp'=2] {'tp'}, dimensions={1}, use_global_device_ids=true | all-gather | bytes 139264 | tf_op jit(solution)/shard_map/all_gather | solution.py:64
  104.8 2.6 fusion.5
  107.6 17.8 %all-gather.6 = f32[16,32,16]{1,2,0:T(8,128)S(1)} all-gather(f32[1,32,16]{1,2,0:T(8,128)S(1)} %bitcast.102), channel_id=4, replica_groups=mesh['tp'=16,'dp'=2] {'tp'}, dimensions={0}, use_global_device_ids=true | all-gather | bytes 34816 | tf_op jit(solution)/shard_map/all_gather | solution.py:76
  127.1 9.3 %all-gather.3 = bf16[1,2048,128]{2,1,0:T(8,128)(2,1)} all-gather(bf16[1,1024,128]{2,1,0:T(8,128)(2,1)S(1)} %get-tuple-element.6), channel_id=5, replica_groups=mesh['tp'=16,'dp'=2] {'dp'}, dimensions={1}, use_global_device_ids=true | all-gather | bytes 786432 | tf_op jit(solution)/shard_map/all_gather | solution.py:37
  136.5 8.3 %all-gather.4 = bf16[1,2048,128]{2,1,0:T(8,128)(2,1)S(1)} all-gather(bf16[1,1024,128]{2,1,0:T(8,128)(2,1)S(1)} %get-tuple-element.8), channel_id=6, replica_groups=mesh['tp'=16,'dp'=2] {'dp'}, dimensions={1}, use_global_device_ids=true | all-gather | bytes 786432 | tf_op jit(solution)/shard_map/all_gather | solution.py:38
  144.8 7.7 %all_gather.68 = bf16[2048,128]{0,1:T(8,128)(2,1)} all-gather(bf16[1024,128]{0,1:T(8,128)(2,1)S(1)} %get-tuple-element.11), channel_id=1, replica_groups=mesh['tp'=16,'dp'=2] {'dp'}, dimensions={0}, use_global_device_ids=true | all-gather | bytes 786432 | tf_op jit(solution)/shard_map/all_gather | solution.py:39
  152.5 7.1 %all_gather.71 = bf16[2048,128]{0,1:T(8,128)(2,1)} all-gather(bf16[1024,128]{0,1:T(8,128)(2,1)S(1)} %get-tuple-element.4), channel_id=1, replica_groups=mesh['tp'=16,'dp'=2] {'dp'}, dimensions={0}, use_global_device_ids=true | all-gather | bytes 786432 | tf_op jit(solution)/shard_map/all_gather | solution.py:40
  159.7 21.5 %reduce-scatter.3.cloned.1.call-done = f32[128,32]{0,1:T(8,128)} async-done(((f32[2048,32]{0,1:T(8,128)}), f32[128,32]{0,1:T(8,128)}) %reduce-scatter.3.cloned.1.call-update) | async-done | bytes 16400 | tf_op jit(solution)/shard_map/reduce_scatter | solution.py:84
  181.9 19.8 %all_gather.63 = bf16[32,2048]{1,0:T(8,128)(2,1)S(1)} all-gather(bf16[32,128]{1,0:T(8,128)(2,1)S(1)} %fusion.47), channel_id=1, replica_groups=mesh['tp'=16,'dp'=2] {'tp'}, dimensions={1}, use_global_device_ids=true | all-gather | bytes 139264 | tf_op jit(solution)/shard_map/all_gather | solution.py:21
  204.4 1.2 convolution_convert_fusion.1
  206.4 17.8 %all_gather.65 = bf16[32,2048]{1,0:T(8,128)(2,1)S(1)} all-gather(bf16[32,128]{1,0:T(8,128)(2,1)S(1)} %get-tuple-element.24), channel_id=1, replica_groups=mesh['tp'=16,'dp'=2] {'tp'}, dimensions={1}, use_global_device_ids=true | all-gather | bytes 139264 | tf_op jit(solution)/shard_map/all_gather | solution.py:63
  224.2 19.1 %all_gather.67 = bf16[32,2048]{1,0:T(8,128)(2,1)S(1)} all-gather(bf16[32,128]{1,0:T(8,128)(2,1)S(1)} %get-tuple-element.25), channel_id=1, replica_groups=mesh['tp'=16,'dp'=2] {'tp'}, dimensions={1}, use_global_device_ids=true | all-gather | bytes 139264 | tf_op jit(solution)/shard_map/all_gather | solution.py:64
  243.7 2.6 fusion.2
  246.5 17.8 %all-gather.7 = f32[16,32,16]{1,2,0:T(8,128)S(1)} all-gather(f32[1,32,16]{1,2,0:T(8,128)S(1)} %bitcast.103), channel_id=7, replica_groups=mesh['tp'=16,'dp'=2] {'tp'}, dimensions={0}, use_global_device_ids=true | all-gather | bytes 34816 | tf_op jit(solution)/shard_map/all_gather | solution.py:76
  265.7 3.5 %multiply_add_fusion.1 = (f32[1,32,16,8,128]{4,3,2,1,0:T(8,128)S(1)}, f32[1,32,16,8,128]{4,3,2,1,0:T(8,128)S(1)}) fusion(f32[2,32,16,8,128]{4,3,2,1,0:T(8,128)} %param.17, f32[32,16,8]{2,1,0:T(8,128)S(1)} %copy.55, f32[32,16,128]{2,1,0:T(8,128)S(1)} %broadcast_subtract_fusion.1, f32[32,16,128]{2,1,0:T(8,128)S(1)} %bitcast.93, f32[32,16,8]{2,1,0:T(8,128)S(1)} %copy.63, ...), kind=kLoop, calls=%fused_computation.12 | loop fusion | flops 3145728 | bytes 9469952 | tf_op jit(solution)/shard_map/add | solution.py:71
  269.3 2.3 pad_maximum_fusion
  271.5 48.4 %reduce-scatter.5.cloned.1.call-done = f32[128,32]{0,1:T(8,128)} async-done(((f32[2048,32]{0,1:T(8,128)}), f32[128,32]{0,1:T(8,128)}) %reduce-scatter.5.cloned.1.call-update) | async-done | bytes 16400 | tf_op jit(solution)/shard_map/reduce_scatter | solution.py:84
  319.9 1.3 fusion.46
  (87 shorter events, 12.5 us)
Async XLA Ops:
  7.2 35.5 %copy-start.3 = (bf16[2,1024,128]{2,1,0:T(8,128)(2,1)S(1)}, bf16[2,1024,128]{2,1,0:T(8,128)(2,1)}, u32[]{:S(2)}) copy-start(bf16[2,1024,128]{2,1,0:T(8,128)(2,1)} %param.13) | copy-start | bytes 1572868
  7.2 174.0 %reduce-scatter.3.cloned.1.call-start = ((), (), s32[]{:S(2)}) async-start(), calls=%async_computation.2 | async-start | bytes 278528 | tf_op jit(solution)/shard_map/reduce_scatter | solution.py:84
  32.8 18.8 %copy-start.4 = (bf16[2,1024,16,8]{1,3,2,0:T(8,128)(2,1)S(1)}, bf16[2,1024,16,8]{1,3,2,0:T(8,128)(2,1)}, u32[]{:S(2)}) copy-start(bf16[2,1024,16,8]{1,3,2,0:T(8,128)(2,1)} %param.14) | copy-start | bytes 1572868
  42.7 16.8 %copy-start.5 = (bf16[2,1024,16,8]{1,3,2,0:T(8,128)(2,1)S(1)}, bf16[2,1024,16,8]{1,3,2,0:T(8,128)(2,1)}, u32[]{:S(2)}) copy-start(bf16[2,1024,16,8]{1,3,2,0:T(8,128)(2,1)} %param.15) | copy-start | bytes 1572868
  51.6 15.4 %copy-start.8 = (f32[2,16,8]{1,2,0:T(8,128)S(1)}, f32[2,16,8]{1,2,0:T(8,128)}, u32[]{:S(2)}) copy-start(f32[2,16,8]{1,2,0:T(8,128)} %param.18) | copy-start | bytes 3076
  51.6 15.6 %copy-start.7 = (f32[2,2048]{1,0:T(2,128)S(1)}, f32[2,2048]{1,0:T(2,128)}, u32[]{:S(2)}) copy-start(f32[2,2048]{1,0:T(2,128)} %param.16) | copy-start | bytes 49156
  104.8 21.1 %copy-start = (bf16[2,16,8,2048]{3,2,1,0:T(8,128)(2,1)S(1)}, bf16[2,16,8,2048]{3,2,1,0:T(8,128)(2,1)}, u32[]{:S(2)}) copy-start(bf16[2,16,8,2048]{3,2,1,0:T(8,128)(2,1)} %param.19) | copy-start | bytes 3145732
  125.9 55.3 %copy-start.6 = (bf16[32,128]{1,0:T(8,128)(2,1)S(1)}, bf16[32,128]{1,0:T(8,128)(2,1)}, u32[]{:S(2)}) copy-start(bf16[32,128]{1,0:T(8,128)(2,1)} %param.10) | copy-start | bytes 24580
  126.9 193.0 %reduce-scatter.5.cloned.1.call-start = ((), (), s32[]{:S(2)}) async-start(), calls=%async_computation.3 | async-start | bytes 278528 | tf_op jit(solution)/shard_map/reduce_scatter | solution.py:84
  144.8 61.0 %copy-start.1 = (bf16[1,2048,128]{2,1,0:T(8,128)(2,1)S(1)}, bf16[1,2048,128]{2,1,0:T(8,128)(2,1)}, u32[]{:S(2)}) copy-start(bf16[1,2048,128]{2,1,0:T(8,128)(2,1)} %all-gather.3) | copy-start | bytes 1572868
  159.7 46.0 %copy-start.2 = (bf16[2048,128]{0,1:T(8,128)(2,1)S(1)}, bf16[2048,128]{0,1:T(8,128)(2,1)}, u32[]{:S(2)}) copy-start(bf16[2048,128]{0,1:T(8,128)(2,1)} %all_gather.71) | copy-start | bytes 1572868
Sparse Core Ops, SparseCore 0:
  127.0 54.0 reduce-scatter.2
  265.8 54.0 reduce-scatter.4
